TPU v7x, 32 devices: a whole 2x2x4 slice. The times are simulated.
32 devices in a mesh: sp: 8 (over z, x), tp: 4 (over y, core).
Axes of the slice: x: 2, y: 2, z: 4, core: 2. Of those that a mesh axis runs over, the one named last changes fastest.
Arguments:
- tokens: bfloat16 [8192, 4096], P('sp'), may hold values from -6 to 6
- input_norm_scale: bfloat16 [4096], replicated, may hold values from 0.099609375 to 1.8984375
- mean_input_weight: bfloat16 [4096, 2048], P('sp', 'tp'), may hold values from -0.09375 to 0.09375
- query_matrix: bfloat16 [4096, 2048], P('sp', 'tp'), may hold values from -0.09375 to 0.09375
- key_matrix: bfloat16 [4096, 2048], P('sp', 'tp'), may hold values from -0.09375 to 0.09375
- value_matrix: bfloat16 [4096, 2048], P('sp', 'tp'), may hold values from -0.09375 to 0.09375
- strength_weight: bfloat16 [4096, 16], P('sp', 'tp'), may hold values from -0.09375 to 0.09375
- decay_input_weight: bfloat16 [4096, 16], P('sp', 'tp'), may hold values from -0.25 to 0.25
- causal_filter_weight: bfloat16 [4, 3, 2048], replicated, may hold values from -3 to 3
- head_decay_logrates: float32 [16], replicated, may hold values from -13.2 to -2.9
- decay_input_shift: float32 [16], replicated, may hold values from -1 to 1
- strength_shift: float32 [16], replicated, may hold values from -5 to -3
- decay_spike: float32 [8192, 16], P('sp', 'tp'), may hold values from -1.3 to 0
- head_norm_scale: bfloat16 [128], replicated, may hold values from 0.099609375 to 1.8984375
- group_mixing_weight: bfloat16 [16, 128, 128], replicated, may hold values from -0.5 to 0.5
- mean_channel_scale: bfloat16 [2048], replicated, may hold values from 0.099609375 to 1.8984375
- mean_output_weight: bfloat16 [2048, 4096], P('tp', 'sp'), may hold values from -0.09375 to 0.09375
- delta_output_weight: bfloat16 [2048, 4096], P('tp', 'sp'), may hold values from -0.09375 to 0.09375
Outputs:
- mixed_out: bfloat16 [8192, 4096], P(('sp', 'tp'))
All inputs are finite; a program needn't handle non-finite values.
Results may differ from a plain program's by a relative error of at most 0.015.
Values may be sent and summed in bfloat16 or wider, within the bound.
A program may use at most 128 MiB of HBM per device.

v0:
```python
import jax
import jax.numpy as jnp
from jax import lax
from jax.sharding import PartitionSpec as P

GROUP_DIM = 128
HEAD_DIM = 128
CONV = 4
BLOCK = 64


EPSILON = 1e-06


def shifted_2(block, axis, distance):
    devices = range(lax.axis_size(axis))
    route = [(i - distance, i) for i in devices if i - distance in devices]
    return lax.ppermute(block, axis, route)


def scale_rows(values, gain_vec):
    squares = jnp.mean(values * values, axis=-1, keepdims=True)
    return values * lax.rsqrt(squares + EPSILON) * gain_vec.astype(jnp.float32)


def unit_rows(values):
    return values * lax.rsqrt(jnp.sum(values * values, axis=-1, keepdims=True) + EPSILON)


def causal_taps(extended, taps, rows_out):
    tap_sum = jnp.zeros((rows_out, taps.shape[1]), jnp.float32)
    for tap_index in range(taps.shape[0]):
        tap_sum = tap_sum + taps[tap_index] * extended[tap_index : tap_index + rows_out]
    return jax.nn.silu(tap_sum)


def pool_means(previous, current, group_ids, positions):
    pool_reach = 15
    rows_out = current.shape[0]
    extended = jnp.concatenate([previous, current], axis=0).astype(jnp.float32)
    window_size = jnp.left_shift(jnp.int32(2), group_ids % 4)
    windowed = jnp.zeros(current.shape, jnp.float32)
    for lag_rows in range(pool_reach + 1):
        shifted = extended[pool_reach - lag_rows : pool_reach - lag_rows + rows_out]
        windowed = windowed + jnp.where(lag_rows < window_size[None, :], shifted, 0.0)
    counts = jnp.minimum(positions[:, None] + 1, window_size[None, :]).astype(jnp.float32)
    return (windowed / counts - extended[pool_reach:]).astype(jnp.bfloat16)


def unit_lower_solve(strict_part, right_side):
    power = strict_part
    solved = right_side - jnp.einsum(
        "nhij,nhjd->nhid", power, right_side, precision=lax.Precision.HIGHEST
    )
    for square_index in range((BLOCK - 1).bit_length() - 1):
        power = jnp.einsum("nhij,nhjk->nhik", power, power, precision=lax.Precision.HIGHEST)
        solved = solved + jnp.einsum(
            "nhij,nhjd->nhid", power, solved, precision=lax.Precision.HIGHEST
        )
    return solved


def block_terms(query, keys, values, decay_logarithm, beta):
    blocks = keys.shape[0] // BLOCK

    def to_blocks(tensor):
        return jnp.swapaxes(tensor.reshape((blocks, BLOCK) + tensor.shape[1:]), 1, 2)

    query_b = to_blocks(query)
    keys_b = to_blocks(keys)
    values_b = to_blocks(values)
    decay_b = to_blocks(decay_logarithm)
    beta_b = to_blocks(beta)
    cumulative = jnp.cumsum(decay_b, axis=-1)
    positions = jnp.arange(BLOCK)
    causal = positions[:, None] >= positions[None, :]
    strict = positions[:, None] > positions[None, :]
    spread = cumulative[..., :, None] - cumulative[..., None, :]
    weights = jnp.where(causal, jnp.exp(jnp.where(causal, spread, 0.0)), 0.0)
    keys_beta = keys_b * beta_b[..., None]
    values_beta = values_b * beta_b[..., None]
    intersection = jnp.einsum("nhid,nhjd->nhij", keys_beta, keys_b, precision=lax.Precision.HIGHEST)
    strict_part = jnp.where(strict, intersection * weights, 0.0)
    right_side = jnp.concatenate([values_beta, keys_beta * jnp.exp(cumulative)[..., None]], axis=-1)
    solved = unit_lower_solve(strict_part, right_side)
    value_depth = values.shape[-1]
    update = solved[..., :value_depth]
    project = solved[..., value_depth:]
    scores = (
        jnp.einsum("nhid,nhjd->nhij", query_b, keys_b, precision=lax.Precision.HIGHEST) * weights
    )
    query_dec = query_b * jnp.exp(cumulative)[..., None]
    keys_dec = keys_b * jnp.exp(cumulative[..., -1:] - cumulative)[..., None]
    carry_decay = jnp.exp(cumulative[..., -1])
    return (scores, query_dec, keys_dec, update, project, carry_decay)


def run_blocks(state, terms):

    def advance(carried, inputs):
        scores, query_dec, keys_dec, update, project, carry_decay = inputs
        fresh = update - jnp.einsum(
            "hcd,hde->hce", project, carried, precision=lax.Precision.HIGHEST
        )
        output = jnp.einsum("hcd,hde->hce", query_dec, carried, precision=lax.Precision.HIGHEST)
        output = output + jnp.einsum("hij,hje->hie", scores, fresh, precision=lax.Precision.HIGHEST)
        carried = carried * carry_decay[:, None, None] + jnp.einsum(
            "hcd,hce->hde", keys_dec, fresh, precision=lax.Precision.HIGHEST
        )
        return (carried, output)

    final_state, outputs = lax.scan(advance, state, terms)
    return outputs


def apply_map(step_map, target):
    return jnp.einsum("hde,hef->hdf", step_map, target, precision=lax.Precision.HIGHEST)


def block_maps(terms, head_count, head_depth):
    scores, query_dec, keys_dec, update, project, carry_decay = terms
    identity = jnp.eye(head_depth, dtype=jnp.float32)
    step_maps = carry_decay[..., None, None] * identity - jnp.einsum(
        "nhcd,nhce->nhde", keys_dec, project, precision=lax.Precision.HIGHEST
    )
    injects = jnp.einsum("nhcd,nhce->nhde", keys_dec, update, precision=lax.Precision.HIGHEST)

    def compose(carried, inputs):
        step_map, inject = inputs
        return ((apply_map(step_map, carried[0]), apply_map(step_map, carried[1]) + inject), None)

    start_maps = (
        jnp.broadcast_to(identity, (head_count, head_depth, head_depth)),
        jnp.zeros((head_count, head_depth, head_depth), jnp.float32),
    )
    composed, unused = lax.scan(compose, start_maps, (step_maps, injects))
    return composed


def per_device(
    tokens,
    input_norm_scale,
    mean_input_weight,
    query_matrix,
    key_matrix,
    value_matrix,
    strength_weight,
    decay_input_weight,
    causal_filter_weight,
    head_decay_logrates,
    decay_input_shift,
    strength_shift,
    decay_spike,
    head_norm_scale,
    group_mixing_weight,
    mean_channel_scale,
    mean_output_weight,
    delta_output_weight,
):
    tok_rows = tokens.shape[0]
    pool_cols = mean_input_weight.shape[1]
    delta_cols = query_matrix.shape[1]
    head_count = strength_weight.shape[1]
    head_depth = delta_cols // head_count
    groups_dev = pool_cols // GROUP_DIM
    tp_index = lax.axis_index("tp")
    sp_index = lax.axis_index("sp")
    normed = scale_rows(tokens.astype(jnp.float32), input_norm_scale).astype(jnp.bfloat16)
    pieces = (
        lax.all_gather(mean_input_weight, "sp", axis=0, tiled=True),
        lax.all_gather(query_matrix, "sp", axis=0, tiled=True),
        lax.all_gather(key_matrix, "sp", axis=0, tiled=True),
        lax.all_gather(value_matrix, "sp", axis=0, tiled=True),
        lax.all_gather(strength_weight, "sp", axis=0, tiled=True),
        lax.all_gather(decay_input_weight, "sp", axis=0, tiled=True),
    )
    wide_part = jnp.concatenate(pieces[:4], axis=1)
    narrow_part = jnp.concatenate(pieces[4:], axis=1)
    wide_sum = jnp.dot(normed, wide_part, preferred_element_type=jnp.float32)
    narrow_sum = jnp.dot(normed, narrow_part, preferred_element_type=jnp.float32)
    pool_raw = wide_sum[:, :pool_cols].astype(jnp.bfloat16)
    qkv_raw = wide_sum[:, pool_cols:].astype(jnp.bfloat16)
    beta_raw = narrow_sum[:, :head_count].astype(jnp.bfloat16)
    decay_unshaped = narrow_sum[:, head_count:].astype(jnp.bfloat16)
    pool_reach = 15
    conv_reach = CONV - 1
    previous_pool, previous_qkv = shifted_2(
        (pool_raw[tok_rows - pool_reach :], qkv_raw[tok_rows - conv_reach :]), "sp", 1
    )
    conv_local = (
        lax.dynamic_slice_in_dim(causal_filter_weight, tp_index * delta_cols, delta_cols, 2)
        .reshape(CONV, 3 * delta_cols)
        .astype(jnp.float32)
    )
    extended_qkv = jnp.concatenate([previous_qkv, qkv_raw], axis=0).astype(jnp.float32)
    convolved = causal_taps(extended_qkv, conv_local, tok_rows)
    query = unit_rows(
        convolved[:, :delta_cols].reshape(tok_rows, head_count, head_depth)
    ) * HEAD_DIM ** (-0.5)
    keys = unit_rows(
        convolved[:, delta_cols : 2 * delta_cols].reshape(tok_rows, head_count, head_depth)
    )
    values = convolved[:, 2 * delta_cols :].reshape(tok_rows, head_count, head_depth)
    rate_logarithm = lax.dynamic_slice_in_dim(
        head_decay_logrates, tp_index * head_count, head_count
    )
    shift_amounts = lax.dynamic_slice_in_dim(decay_input_shift, tp_index * head_count, head_count)
    strength_offsets = lax.dynamic_slice_in_dim(strength_shift, tp_index * head_count, head_count)
    beta = jax.nn.sigmoid(beta_raw.astype(jnp.float32) + strength_offsets)
    decay_logarithm = (
        -jnp.exp(rate_logarithm)
        * jax.nn.softplus(decay_unshaped.astype(jnp.float32) + shift_amounts)
        + decay_spike
    )
    terms = block_terms(query, keys, values, decay_logarithm, beta)
    transfer_map, offset_map = block_maps(terms, head_count, head_depth)

    def hop(step_count, incoming):
        advanced = apply_map(transfer_map, incoming) + offset_map
        return shifted_2(advanced.astype(jnp.bfloat16), "sp", 1).astype(advanced.dtype)

    incoming = lax.fori_loop(0, lax.axis_size("sp") - 1, hop, jnp.zeros_like(offset_map))
    outputs = run_blocks(incoming, terms)
    delta_rows = jnp.swapaxes(outputs, 1, 2).reshape(tok_rows, head_count, head_depth)
    delta_mixed = (
        scale_rows(delta_rows, head_norm_scale).astype(jnp.bfloat16).reshape(tok_rows, delta_cols)
    )
    group_ids = tp_index * groups_dev + jnp.arange(pool_cols) // GROUP_DIM
    positions = sp_index * tok_rows + jnp.arange(tok_rows)
    pool_diff = pool_means(previous_pool, pool_raw, group_ids, positions)
    local_mix = lax.dynamic_slice_in_dim(group_mixing_weight, tp_index * groups_dev, groups_dev, 0)
    pooled = jnp.einsum(
        "tgc,gcd->tgd",
        pool_diff.reshape(tok_rows, groups_dev, GROUP_DIM),
        local_mix,
        preferred_element_type=jnp.float32,
    )
    pool_scale = lax.dynamic_slice_in_dim(mean_channel_scale, tp_index * pool_cols, pool_cols)
    pool_mixed = (pooled.reshape(tok_rows, pool_cols) * pool_scale.astype(jnp.float32)).astype(
        jnp.bfloat16
    )
    mixed = jnp.concatenate([pool_mixed, delta_mixed], axis=1)
    pool_weight_rows, delta_weight_rows = (
        lax.all_gather(mean_output_weight, "sp", axis=1, tiled=True),
        lax.all_gather(delta_output_weight, "sp", axis=1, tiled=True),
    )
    out_weight = jnp.concatenate([pool_weight_rows, delta_weight_rows], axis=0)
    return lax.psum_scatter(
        jnp.dot(mixed, out_weight, preferred_element_type=jnp.float32).astype(jnp.bfloat16),
        "tp",
        scatter_dimension=0,
        tiled=True,
    )


def solution(mesh):
    return jax.shard_map(
        per_device,
        mesh=mesh,
        in_specs=(
            P("sp", None),
            P(),
            P("sp", "tp"),
            P("sp", "tp"),
            P("sp", "tp"),
            P("sp", "tp"),
            P("sp", "tp"),
            P("sp", "tp"),
            P(),
            P(),
            P(),
            P(),
            P("sp", "tp"),
            P(),
            P(),
            P(),
            P("tp", "sp"),
            P("tp", "sp"),
        ),
        out_specs=P(("sp", "tp"), None),
        check_vma=False,
    )
```

profile of v0, /device:TPU:0, one launch (start us, length us, event | category | flops | bytes accessed | tf_op | source)
XLA Modules:
  0.0 758.3 jit_solution(1002801814942155716)
XLA Ops:
  16.0 5.3 fusion.32
  21.3 33.6 %all_gather.28 = bf16[4096,4]{0,1:T(4,128)(2,1)S(1)} all-gather(bf16[512,4]{0,1:T(4,128)(2,1)S(1)} %copy-done.11), channel_id=1, replica_groups=mesh['sp'=8,'tp'=4] {'sp'}, dimensions={0}, use_global_device_ids=true | all-gather | bytes 36864 | tf_op jit(solution)/shard_map/all_gather | solution.py:174
  55.0 31.6 %all_gather.29 = bf16[4096,4]{0,1:T(4,128)(2,1)S(1)} all-gather(bf16[512,4]{0,1:T(4,128)(2,1)S(1)} %copy-done.12), channel_id=1, replica_groups=mesh['sp'=8,'tp'=4] {'sp'}, dimensions={0}, use_global_device_ids=true | all-gather | bytes 36864 | tf_op jit(solution)/shard_map/all_gather | solution.py:175
  92.6 66.7 %all-gather.13.cloned.1.call-done = bf16[4096,512]{1,0:T(8,128)(2,1)} async-done(((bf16[512,512]{1,0:T(8,128)(2,1)}), bf16[4096,512]{1,0:T(8,128)(2,1)}) %all-gather.13.cloned.1.call-update) | async-done | bytes 4194320 | tf_op jit(solution)/shard_map/all_gather | solution.py:173
  159.3 73.5 %all-gather.7.cloned.1.call-done = bf16[4096,512]{1,0:T(8,128)(2,1)} async-done(((bf16[512,512]{1,0:T(8,128)(2,1)}), bf16[4096,512]{1,0:T(8,128)(2,1)}) %all-gather.7.cloned.1.call-update) | async-done | bytes 4194320 | tf_op jit(solution)/shard_map/all_gather | solution.py:170
  232.7 73.3 %all-gather.9.cloned.1.call-done = bf16[4096,512]{1,0:T(8,128)(2,1)} async-done(((bf16[512,512]{1,0:T(8,128)(2,1)}), bf16[4096,512]{1,0:T(8,128)(2,1)}) %all-gather.9.cloned.1.call-update) | async-done | bytes 4194320 | tf_op jit(solution)/shard_map/all_gather | solution.py:171
  306.1 27.1 %fusion.53 = bf16[1024,2048]{1,0:T(8,128)(2,1)} fusion(bf16[4096,512]{1,0:T(8,128)(2,1)} %all-gather.13.cloned.1.call-done, bf16[4096,512]{1,0:T(8,128)(2,1)} %all-gather.11.cloned.1.call-done, bf16[4096,512]{1,0:T(8,128)(2,1)} %all-gather.9.cloned.1.call-done, bf16[4096,512]{1,0:T(8,128)(2,1)} %all-gather.7.cloned.1.call-done, ...), kind=kOutput, calls=%fused_computation.66 | convolution fusion | flops 17265852416 | bytes 29380608 | tf_op jit(solution)/shard_map/dot_general | solution.py:179
  340.1 5.0 collective-permute-start.1
  349.9 4.5 slice_multiply_fusion.4
  378.1 4.6 multiply_select_fusion
  387.4 5.5 fusion.93
  392.9 7.3 multiply_multiply_fusion
  400.2 4.3 fusion.57
  404.5 4.8 convolution_add_fusion.6
  411.7 4.7 fusion.145
  418.8 4.8 convolution_add_fusion.5
  425.9 4.5 fusion.148
  430.4 4.8 convolution_add_fusion.4
  437.9 8.5 %fusion.138 = f32[16,4,128,128]{3,2,1,0:T(8,128)} fusion(f32[16,4,64,128]{3,2,1,0:T(8,128)S(1)} %get-tuple-element.411, f32[16,4,64,256]{3,2,1,0:T(8,128)S(1)} %convolution_add_fusion.4), kind=kOutput, calls=%fused_computation.210 | convolution fusion | flops 805306368 | bytes 8388608 | tf_op jit(solution)/shard_map/nhcd,nhce->nhde/dot_general | solution.py:126
  446.4 8.8 %multiply_subtract_fusion = f32[16,4,128,128]{3,2,1,0:T(8,128)} fusion(f32[16,4,64,128]{3,2,1,0:T(8,128)S(1)} %get-tuple-element.411, f32[128,128]{1,0:T(8,128)S(1)} %fusion.120, f32[16,4]{1,0:T(8,128)S(1)} %copy.88, f32[16,4,64,256]{3,2,1,0:T(8,128)S(1)} %convolution_add_fusion.4), kind=kOutput, calls=%fused_computation.65 | convolution fusion | flops 807403520 | bytes 8462336 | tf_op jit(solution)/shard_map/nhcd,nhce->nhde/dot_general | solution.py:123
  455.2 45.7 %while.37 = (s32[]{:T(128)}, f32[4,128,128]{2,1,0:T(8,128)S(1)}, f32[4,128,128]{2,1,0:T(8,128)S(1)}, f32[16,4,128,128]{3,2,1,0:T(8,128)}, f32[16,4,128,128]{3,2,1,0:T(8,128)}, /*index=5*/s32[]{:T(128)}, s32[]{:T(128)}) while((s32[]{:T(128)}, f32[4,128,128]{2,1,0:T(8,128)S(1)}, f32[4,128,128]{2,1,0:T(8,128)S(1)}, ...), condition=%wide.region_4.5_spmd.clone, body=%wide.region_3.4_spmd.clone.sunk | while | flops 201457664 | bytes 2885207 | solution.py:136
  501.0 61.3 %while.38 = (s32[]{:T(128)}, f32[4,128,128]{2,1,0:T(8,128)S(1)}, f32[4,128,128]{2,1,0:T(8,128)S(1)}, f32[4,128,128]{2,1,0:T(8,128)S(1)}, s32[]{:T(128)}, /*index=5*/s32[]{:T(128)}) while((s32[]{:T(128)}, f32[4,128,128]{2,1,0:T(8,128)S(1)}, f32[4,128,128]{2,1,0:T(8,128)S(1)}, f32[4,128,128]{2,1,0:T(8,128)S(1)}, s32[]{:T(128)}, ...), condition=%wide.region_6.7_spmd.clone, body=%wide.region_5.6_spmd.clone.sunk | while | flops 100925440 | bytes 1835127 | solution.py:222
  507.2 5.1 collective-permute-start
  515.5 5.6 collective-permute-start
  524.2 6.0 collective-permute-start
  533.4 6.0 collective-permute-start
  543.0 6.3 collective-permute-start
  553.7 5.8 collective-permute-start
  562.3 81.5 %while.36 = (s32[]{:T(128)}, f32[4,128,128]{2,1,0:T(8,128)S(1)}, f32[16,4,64,128]{3,2,1,0:T(8,128)}, f32[16,4]{1,0:T(8,128)S(1)}, f32[16,4,64,128]{3,2,1,0:T(8,1...) while((s32[]{:T(128)}, f32[4,128,128]{2,1,0:T(8,128)S(1)}, ...), condition=%wide.region_9.10_spmd, body=%wide.region_8.9_spmd.sunk | while | flops 176357376 | bytes 2493581 | solution.py:112
  652.1 8.1 %fusion.107 = f32[4,128,1024]{2,1,0:T(8,128)} fusion(bf16[16,128,128]{2,1,0:T(8,128)(2,1)S(1)} %copy-done, s32[]{:T(128)S(6)} %select_n.189, s32[512]{0:T(512)S(1)} %copy-done.13, s32[1024]{0:T(1024)S(1)} %add_add_fusion, f32[1039,512]{1,0:T(8,128)S(1)} %maximum_convert_fusion.1, pred[512]{0:T(512)(128)(4,1)S(1)} %copy-done.18, ...), kind=kOutput, calls=%fused_computation.135 | convolution fusion | flops 153092096 | bytes 35796996 | tf_op jit(solution)/shard_map/tgc,gcd->tgd/dot_general | solution.py:232
  663.4 13.8 %fusion.47 = bf16[1024,4096]{1,0:T(8,128)(2,1)} fusion(bf16[512,4096]{1,0:T(8,128)(2,1)} %all-gather.17.cloned.1.call-done, bf16[512,4096]{1,0:T(8,128)(2,1)} %all-gather.15.cloned.1.call-done, bf16[1024,512]{1,0:T(8,128)(2,1)} %fusion.67, bf16[1024,512]{1,0:T(8,128)(2,1)} %multiply_convert_fusion), kind=kOutput, calls=%fused_computation.55 | convolution fusion | flops 8615100416 | bytes 18874368 | tf_op jit(solution)/shard_map/dot_general | solution.py:249
  677.3 73.7 %reduce-scatter.2.cloned.1.call-done = bf16[256,4096]{1,0:T(8,128)(2,1)} async-done(((bf16[1024,4096]{1,0:T(8,128)(2,1)}), bf16[256,4096]{1,0:T(8,128)(2,1)}) %reduce-scatter.2.cloned.1.call-update) | async-done | bytes 2097168 | tf_op jit(solution)/shard_map/reduce_scatter | solution.py:248
  (331 shorter events, 227.9 us)
Async XLA Ops:
  6.5 645.4 %copy-start = (bf16[16,128,128]{2,1,0:T(8,128)(2,1)S(1)}, bf16[16,128,128]{2,1,0:T(8,128)(2,1)}, u32[]{:S(2)}) copy-start(bf16[16,128,128]{2,1,0:T(8,128)(2,1)} %param.38) | copy-start | bytes 1572868
  6.5 9.2 %copy-start.14 = (f32[16]{0:T(128)S(1)}, f32[16]{0:T(128)}, u32[]{:S(2)}) copy-start(f32[16]{0:T(128)} %param.34) | copy-start | bytes 196
  6.5 9.3 %copy-start.15 = (f32[16]{0:T(128)S(1)}, f32[16]{0:T(128)}, u32[]{:S(2)}) copy-start(f32[16]{0:T(128)} %param.35) | copy-start | bytes 196
  6.5 9.4 %copy-start.16 = (f32[16]{0:T(128)S(1)}, f32[16]{0:T(128)}, u32[]{:S(2)}) copy-start(f32[16]{0:T(128)} %param.33) | copy-start | bytes 196
  6.5 9.5 %copy-start.8 = (bf16[4096]{0:T(1024)(128)(2,1)S(1)}, bf16[4096]{0:T(1024)(128)(2,1)}, u32[]{:S(2)}) copy-start(bf16[4096]{0:T(1024)(128)(2,1)} %param.25) | copy-start | bytes 24580
  6.5 86.0 %all-gather.11.cloned.1.call-start = ((), (), s32[]{:S(2)}) async-start(), calls=%async_computation.3 | async-start | bytes 4718592 | tf_op jit(solution)/shard_map/all_gather | solution.py:172
  7.3 152.0 %all-gather.13.cloned.1.call-start = ((), (), s32[]{:S(2)}) async-start(), calls=%async_computation.4 | async-start | bytes 4718592 | tf_op jit(solution)/shard_map/all_gather | solution.py:173
  8.0 224.7 %all-gather.7.cloned.1.call-start = ((), (), s32[]{:S(2)}) async-start(), calls=%async_computation.1 | async-start | bytes 4718592 | tf_op jit(solution)/shard_map/all_gather | solution.py:170
  8.8 297.3 %all-gather.9.cloned.1.call-start = ((), (), s32[]{:S(2)}) async-start(), calls=%async_computation.2 | async-start | bytes 4718592 | tf_op jit(solution)/shard_map/all_gather | solution.py:171
  9.3 654.1 %all-gather.15.cloned.1.call-start = ((), (), s32[]{:S(2)}) async-start(), calls=%async_computation.5 | async-start | bytes 4718592 | tf_op jit(solution)/shard_map/all_gather | solution.py:244
  9.9 653.5 %all-gather.17.cloned.1.call-start = ((), (), s32[]{:S(2)}) async-start(), calls=%async_computation.6 | async-start | bytes 4718592 | tf_op jit(solution)/shard_map/all_gather | solution.py:245
  10.5 740.5 %reduce-scatter.2.cloned.1.call-start = ((), (), s32[]{:S(2)}) async-start(), calls=%async_computation.7 | async-start | bytes 10485760 | tf_op jit(solution)/shard_map/reduce_scatter | solution.py:248
  16.0 5.3 copy-start.11
  16.0 39.0 %copy-start.12 = (bf16[512,4]{0,1:T(4,128)(2,1)S(1)}, bf16[512,4]{0,1:T(4,128)(2,1)}, u32[]{:S(2)}) copy-start(bf16[512,4]{0,1:T(4,128)(2,1)} %param.31) | copy-start | bytes 12292
  16.0 70.6 %copy-start.5 = (bf16[1024,4096]{1,0:T(8,128)(2,1)S(1)}, bf16[1024,4096]{1,0:T(8,128)(2,1)}, u32[]{:S(2)}) copy-start(bf16[1024,4096]{1,0:T(8,128)(2,1)} %param.24) | copy-start | bytes 25165828
  86.6 2.4 copy-start.7
  86.6 4.6 copy-start.17
  333.9 11.2 %collective-permute-start.2 = (bf16[3,1536]{1,0:T(4,128)(2,1)S(1)}, bf16[3,1536]{1,0:T(4,128)(2,1)S(1)}, u32[]{:S(2)}, u32[]{:S(2)}) collective-permute-start(bf16[3,1536]{1,0:T(4,128)(2,1)S(1)} %slice.177), channel_id=1, source_target_pairs={{0,4},{4,8},{8,12},{12,16},{16,20},{20,24},{24,28},{1,5},{5,9},{9,... | collective-permute-start | bytes 27656 | tf_op jit(solution)/shard_map/ppermute | solution.py:18
  337.3 7.8 %slice-start = ((bf16[1024,2048]{1,0:T(8,128)(2,1)}), bf16[1024,1536]{1,0:T(8,128)(2,1)S(1)}, s32[]{:S(2)}) async-start(bf16[1024,2048]{1,0:T(8,128)(2,1)} %fusion.53), calls=%async_computation.8 | async-start | bytes 6291456 | tf_op jit(solution)/shard_map/slice | solution.py:182
  340.1 310.7 %collective-permute-start.1 = (bf16[15,512]{1,0:T(8,128)(2,1)}, bf16[15,512]{1,0:T(8,128)(2,1)}, u32[]{:S(2)}, u32[]{:S(2)}) collective-permute-start(bf16[15,512]{1,0:T(8,128)(2,1)} %slice.156), channel_id=1, source_target_pairs={{0,4},{4,8},{8,12},{12,16},{16,20},{20,24},{24,28},{1,5},{5,9},{9,... | collective-permute-start | bytes 46088 | tf_op jit(solution)/shard_map/ppermute | solution.py:18
  361.6 25.8 %copy-start.2 = (f32[16,64,4,128]{3,2,1,0:T(4,128)}, f32[16,64,4,128]{3,2,1,0:T(4,128)S(1)}, u32[]{:S(2)}) copy-start(f32[16,64,4,128]{3,2,1,0:T(4,128)S(1)} %reshape.220) | copy-start | bytes 6291460
  374.9 3.1 copy-start.9
  385.0 2.4 copy-start.3
  387.4 5.5 copy-start.4
  501.4 4.4 collective-permute-start
  507.2 7.0 collective-permute-start
  515.5 7.4 collective-permute-start
  524.2 7.9 %collective-permute-start = (bf16[4,128,128]{2,1,0:T(8,128)(2,1)S(1)}, bf16[4,128,128]{2,1,0:T(8,128)(2,1)}, u32[]{:S(2)}, u32[]{:S(2)}) collective-permute-start(bf16[4,128,128]{2,1,0:T(8,128)(2,1)S(1)} %fusion.215), channel_id=1, source_target_pairs={{0,4},{4,8},{8,12},{12,16},{16,20},{20,24},{24,28},{1,5},{5,9},{9,... | collective-permute-start | bytes 393224 | tf_op jit(solution)/shard_map/while/body/eval_jaxpr/ppermute | solution.py:18
  533.4 8.2 %collective-permute-start = (bf16[4,128,128]{2,1,0:T(8,128)(2,1)S(1)}, bf16[4,128,128]{2,1,0:T(8,128)(2,1)}, u32[]{:S(2)}, u32[]{:S(2)}) collective-permute-start(bf16[4,128,128]{2,1,0:T(8,128)(2,1)S(1)} %fusion.215), channel_id=1, source_target_pairs={{0,4},{4,8},{8,12},{12,16},{16,20},{20,24},{24,28},{1,5},{5,9},{9,... | collective-permute-start | bytes 393224 | tf_op jit(solution)/shard_map/while/body/eval_jaxpr/ppermute | solution.py:18
  543.0 9.5 %collective-permute-start = (bf16[4,128,128]{2,1,0:T(8,128)(2,1)S(1)}, bf16[4,128,128]{2,1,0:T(8,128)(2,1)}, u32[]{:S(2)}, u32[]{:S(2)}) collective-permute-start(bf16[4,128,128]{2,1,0:T(8,128)(2,1)S(1)} %fusion.215), channel_id=1, source_target_pairs={{0,4},{4,8},{8,12},{12,16},{16,20},{20,24},{24,28},{1,5},{5,9},{9,... | collective-permute-start | bytes 393224 | tf_op jit(solution)/shard_map/while/body/eval_jaxpr/ppermute | solution.py:18
  553.7 7.6 %collective-permute-start = (bf16[4,128,128]{2,1,0:T(8,128)(2,1)S(1)}, bf16[4,128,128]{2,1,0:T(8,128)(2,1)}, u32[]{:S(2)}, u32[]{:S(2)}) collective-permute-start(bf16[4,128,128]{2,1,0:T(8,128)(2,1)S(1)} %fusion.215), channel_id=1, source_target_pairs={{0,4},{4,8},{8,12},{12,16},{16,20},{20,24},{24,28},{1,5},{5,9},{9,... | collective-permute-start | bytes 393224 | tf_op jit(solution)/shard_map/while/body/eval_jaxpr/ppermute | solution.py:18
  643.8 2.6 copy-start.6
  (20 other events, 26.6 us)
Sparse Core Ops, SparseCore 0:
  9.5 76.2 all-gather.10
  87.9 71.2 all-gather.12
  161.4 71.3 all-gather.6
  234.7 71.3 all-gather.8
  308.0 73.5 all-gather.14
  383.5 72.8 all-gather.16
  677.4 73.5 reduce-scatter.1
where the time goes:
time: 769 us; the launch traced here: 758 us
  waiting for transfers between devices  305 us (40%)
  matrix products  246 us (32%)
  blocking collectives  65.2 us (8%)
  other arithmetic  52.1 us (7%)
  starting transfers between devices  45.1 us (6%)
  local copies, waits for them, and re-layouts  27.6 us (4%)
  between operations  14.7 us (2%)
    reduce_scatter x1, waiting for transfers between devices, per_device(): lax.psum_scatter(jnp.dot(mixed, out_weight, preferred_element_type=jnp.fl...  73.7 us
    all_gather x1, waiting for transfers between devices, per_device(): lax.all_gather(mean_input_weight, 'sp', axis=0, tiled=True)  73.5 us
    all_gather x1, waiting for transfers between devices, per_device(): lax.all_gather(query_matrix, 'sp', axis=0, tiled=True)  73.3 us
    all_gather x1, waiting for transfers between devices, per_device(): lax.all_gather(value_matrix, 'sp', axis=0, tiled=True)  66.7 us
    dot_general x39, matrix products, apply_map(): jnp.einsum('hde,hef->hdf', step_map, target, precision=lax.Precision.HIGH...  47.1 us
    ppermute x9, starting transfers between devices, shifted_2(): return lax.ppermute(block, axis, route)  44.8 us
    all_gather x1, blocking collectives, per_device(): lax.all_gather(strength_weight, 'sp', axis=0, tiled=True)  33.6 us
    all_gather x1, blocking collectives, per_device(): lax.all_gather(decay_input_weight, 'sp', axis=0, tiled=True)  31.6 us
  transfers between devices with their start and end apart: 16, of which 11 were waited for; matrix products, arithmetic and copies ran while one was open for 41% of the time, Pallas kernels for 0%

commit v1 on v0

v1 whole, which is shorter than its diff:
```python
import jax
import jax.numpy as jnp
from jax import lax
from jax.experimental import pallas as pl
from jax.experimental.pallas import tpu as pltpu
from jax.sharding import PartitionSpec as P

GROUP_DIM = 128
HEAD_DIM = 128
CONV = 4
BLOCK = 64


EPSILON = 1e-06


def shifted_2(block, axis, distance):
    devices = range(lax.axis_size(axis))
    route = [(i - distance, i) for i in devices if i - distance in devices]
    return lax.ppermute(block, axis, route)


def scale_rows(values, gain_vec):
    squares = jnp.mean(values * values, axis=-1, keepdims=True)
    return values * lax.rsqrt(squares + EPSILON) * gain_vec.astype(jnp.float32)


def pool_means(previous, current, group_ids, positions):
    pool_reach = 15
    rows_out = current.shape[0]
    extended = jnp.concatenate([previous, current], axis=0).astype(jnp.float32)
    window_size = jnp.left_shift(jnp.int32(2), group_ids % 4)
    windowed = jnp.zeros(current.shape, jnp.float32)
    for lag_rows in range(pool_reach + 1):
        shifted = extended[pool_reach - lag_rows : pool_reach - lag_rows + rows_out]
        windowed = windowed + jnp.where(lag_rows < window_size[None, :], shifted, 0.0)
    counts = jnp.minimum(positions[:, None] + 1, window_size[None, :]).astype(jnp.float32)
    return (windowed / counts - extended[pool_reach:]).astype(jnp.bfloat16)


BF16 = jnp.bfloat16
F32 = jnp.float32
HALO = 8


def dot(left, right):
    return jnp.dot(left.astype(BF16), right.astype(BF16), preferred_element_type=F32)


def dot_nt(left, right):
    return lax.dot_general(
        left.astype(BF16),
        right.astype(BF16),
        (((1,), (1,)), ((), ())),
        preferred_element_type=F32,
    )


def dot_tn(left, right):
    return lax.dot_general(
        left.astype(BF16),
        right.astype(BF16),
        (((0,), (0,)), ((), ())),
        preferred_element_type=F32,
    )


def unit_rows(values):
    return values * lax.rsqrt(jnp.sum(values * values, axis=-1, keepdims=True) + EPSILON)


def delta_kernel(heads, depth, chunk, *refs):
    (q_ref, k_ref, v_ref, hq_ref, hk_ref, hv_ref, tap_ref, beta_ref, decay_ref) = refs[:9]
    out_ref, eff_ref, state_ref, carry, halo = refs[9:]
    step = pl.program_id(0)
    width = heads * depth
    row = lax.broadcasted_iota(jnp.int32, (chunk, chunk), 0)
    col = lax.broadcasted_iota(jnp.int32, (chunk, chunk), 1)
    causal = row >= col
    strict = row > col
    eye = jnp.where(row == col, 1.0, 0.0)
    lane = lax.broadcasted_iota(jnp.int32, (depth, 2 * depth), 1)
    sub = lax.broadcasted_iota(jnp.int32, (depth, 2 * depth), 0)

    @pl.when(step == 0)
    def _():
        for h in range(heads):
            carry[h] = jnp.where(lane == sub + depth, 1.0, 0.0)
        halo[0] = hq_ref[...].astype(F32)
        halo[1] = hk_ref[...].astype(F32)
        halo[2] = hv_ref[...].astype(F32)

    convolved = []
    for r, ref in enumerate((q_ref, k_ref, v_ref)):
        current = ref[...].astype(F32)
        extended = jnp.concatenate([halo[r], current], axis=0)
        halo[r] = current[chunk - HALO :]
        total = jnp.zeros((chunk, width), F32)
        for i in range(CONV):
            start = HALO - (CONV - 1) + i
            taps = tap_ref[i, r : r + 1, :].astype(F32)
            total = total + taps * extended[start : start + chunk]
        convolved.append(total / (1.0 + jnp.exp(-total)))
    tri = jnp.where(causal, 1.0, 0.0)
    decay = decay_ref[...]
    cum_cols = jnp.dot(tri, decay, preferred_element_type=F32, precision=lax.Precision.HIGHEST)
    cum_rows = lax.dot_general(
        decay,
        tri,
        (((0,), (1,)), ((), ())),
        preferred_element_type=F32,
        precision=lax.Precision.HIGHEST,
    )
    base = min(16, chunk)
    hs = range(heads)
    q = [unit_rows(convolved[0][:, h * depth : (h + 1) * depth]) * depth ** (-0.5) for h in hs]
    k = [unit_rows(convolved[1][:, h * depth : (h + 1) * depth]) for h in hs]
    v = [convolved[2][:, h * depth : (h + 1) * depth] for h in hs]
    cum = [cum_cols[:, h : h + 1] for h in hs]
    last = [cum_cols[chunk - 1 : chunk, h : h + 1] for h in hs]
    beta = [beta_ref[:, h : h + 1] for h in hs]
    weights = [
        jnp.where(causal, jnp.exp(jnp.where(causal, cum[h] - cum_rows[h : h + 1, :], 0.0)), 0.0)
        for h in hs
    ]
    kb = [k[h] * beta[h] for h in hs]
    lower = [jnp.where(strict, dot_nt(kb[h], k[h]) * weights[h], 0.0) for h in hs]
    power = [jnp.where(row // base == col // base, lower[h], 0.0) for h in hs]
    inverse = [eye - power[h] for h in hs]
    reach = 2
    while reach < base:
        power = [dot(power[h], power[h]) for h in hs]
        inverse = [inverse[h] + dot(inverse[h], power[h]) for h in hs]
        reach *= 2
    size = base
    while size < chunk:
        pair = (row // (2 * size) == col // (2 * size)) & (row // size != col // size)
        right = [dot(jnp.where(pair, lower[h], 0.0), inverse[h]) for h in hs]
        inverse = [inverse[h] - dot(inverse[h], right[h]) for h in hs]
        size *= 2
    grow = [jnp.exp(cum[h]) for h in hs]
    sides = [jnp.concatenate([v[h] * beta[h], kb[h] * grow[h]], axis=1) for h in hs]
    solved = [dot(inverse[h], sides[h]) for h in hs]
    scores = [dot_nt(q[h], k[h]) * weights[h] for h in hs]
    kd = [k[h] * jnp.exp(last[h] - cum[h]) for h in hs]
    zeros = jnp.zeros((chunk, depth), F32)
    state = [carry[h] for h in hs]
    fresh = [
        jnp.concatenate([solved[h][:, :depth], zeros], axis=1) - dot(solved[h][:, depth:], state[h])
        for h in hs
    ]
    outs = [dot(q[h] * grow[h], state[h]) + dot(scores[h], fresh[h]) for h in hs]
    for h in hs:
        carry[h] = state[h] * jnp.exp(last[h]) + dot_tn(kd[h], fresh[h])
        out_ref[:, h * depth : (h + 1) * depth] = outs[h][:, :depth]
        eff_ref[:, h * depth : (h + 1) * depth] = outs[h][:, depth:].astype(BF16)
        state_ref[h] = carry[h]


def delta_pass(q, k, v, hq, hk, hv, taps, beta, decay, depth):
    rows, width = q.shape
    heads = beta.shape[1]
    chunk = min(128, rows)
    whole = lambda shape: pl.BlockSpec(shape, lambda i: (0,) * len(shape))
    tile = pl.BlockSpec((chunk, width), lambda i: (i, 0))
    slim = pl.BlockSpec((chunk, heads), lambda i: (i, 0))
    return pl.pallas_call(
        lambda *refs: delta_kernel(heads, depth, chunk, *refs),
        grid=(rows // chunk,),
        in_specs=[tile] * 3 + [whole(hq.shape)] * 3 + [whole(taps.shape), slim, slim],
        out_specs=[tile, tile, whole((heads, depth, 2 * depth))],
        out_shape=[
            jax.ShapeDtypeStruct((rows, width), F32),
            jax.ShapeDtypeStruct((rows, width), BF16),
            jax.ShapeDtypeStruct((heads, depth, 2 * depth), F32),
        ],
        scratch_shapes=[
            pltpu.VMEM((heads, depth, 2 * depth), F32),
            pltpu.VMEM((3, HALO, width), F32),
        ],
        compiler_params=pltpu.CompilerParams(
            dimension_semantics=("arbitrary",), vmem_limit_bytes=32 * 1024 * 1024
        ),
        cost_estimate=pl.CostEstimate(
            flops=rows * width * 4096, bytes_accessed=rows * width * 12, transcendentals=0
        ),
    )(q, k, v, hq, hk, hv, taps, beta, decay)


def finish_kernel(heads, depth, out_ref, eff_ref, state_ref, gain_ref, mixed_ref):
    gain = gain_ref[...].astype(F32)
    for h in range(heads):
        cols = slice(h * depth, (h + 1) * depth)
        raw = out_ref[:, cols] + dot(eff_ref[:, cols], state_ref[h])
        scale = lax.rsqrt(jnp.mean(raw * raw, axis=-1, keepdims=True) + EPSILON)
        mixed_ref[:, cols] = (raw * scale * gain).astype(BF16)


def finish_pass(out, eff, incoming, gain):
    rows, width = out.shape
    heads, depth = incoming.shape[:2]
    chunk = min(256, rows)
    tile = pl.BlockSpec((chunk, width), lambda i: (i, 0))
    return pl.pallas_call(
        lambda *refs: finish_kernel(heads, depth, *refs),
        grid=(rows // chunk,),
        in_specs=[
            tile,
            tile,
            pl.BlockSpec(incoming.shape, lambda i: (0, 0, 0)),
            pl.BlockSpec((1, depth), lambda i: (0, 0)),
        ],
        out_specs=tile,
        out_shape=jax.ShapeDtypeStruct((rows, width), BF16),
        compiler_params=pltpu.CompilerParams(dimension_semantics=("arbitrary",)),
    )(out, eff, incoming, gain.reshape(1, depth))


def earlier_state(state, depth):
    def compose(later, earlier):
        pushed = jnp.einsum(
            "hde,hef->hdf", later[..., depth:].astype(BF16), earlier, preferred_element_type=F32
        )
        own = jnp.concatenate([later[..., :depth], jnp.zeros_like(later[..., depth:])], axis=-1)
        return own + pushed

    held = shifted_2(state.astype(BF16), "sp", 1)
    count = lax.axis_size("sp")
    distance = 1
    while distance < count - 1:
        sent = held if 2 * distance < count - 1 else held[..., :depth]
        arrived = shifted_2(sent, "sp", distance)
        if 2 * distance < count - 1:
            held = compose(held.astype(F32), arrived).astype(BF16)
        else:
            held = held[..., :depth].astype(F32) + jnp.einsum(
                "hde,hef->hdf", held[..., depth:], arrived, preferred_element_type=F32
            )
        distance *= 2
    return held[..., :depth].astype(BF16)


def per_device(
    tokens,
    input_norm_scale,
    mean_input_weight,
    query_matrix,
    key_matrix,
    value_matrix,
    strength_weight,
    decay_input_weight,
    causal_filter_weight,
    head_decay_logrates,
    decay_input_shift,
    strength_shift,
    decay_spike,
    head_norm_scale,
    group_mixing_weight,
    mean_channel_scale,
    mean_output_weight,
    delta_output_weight,
):
    tok_rows = tokens.shape[0]
    pool_cols = mean_input_weight.shape[1]
    delta_cols = query_matrix.shape[1]
    head_count = strength_weight.shape[1]
    head_depth = delta_cols // head_count
    groups_dev = pool_cols // GROUP_DIM
    tp_index = lax.axis_index("tp")
    sp_index = lax.axis_index("sp")
    normed = scale_rows(tokens.astype(jnp.float32), input_norm_scale).astype(jnp.bfloat16)
    narrow = lax.all_gather(
        jnp.concatenate([strength_weight, decay_input_weight], axis=1), "sp", axis=0, tiled=True
    )
    project = lambda weight: jnp.dot(normed, weight, preferred_element_type=F32).astype(BF16)
    gather = lambda weight: lax.all_gather(weight, "sp", axis=0, tiled=True)
    key_raw = project(gather(key_matrix))
    query_raw = project(gather(query_matrix))
    value_raw = project(gather(value_matrix))
    pool_raw = project(gather(mean_input_weight))
    narrow_raw = project(narrow)
    beta_raw = narrow_raw[:, :head_count]
    decay_unshaped = narrow_raw[:, head_count:]
    pool_reach = 15
    halos = shifted_2(
        tuple(raw[tok_rows - HALO :] for raw in (query_raw, key_raw, value_raw)), "sp", 1
    )
    previous_pool = shifted_2(pool_raw[tok_rows - pool_reach :], "sp", 1)
    taps = lax.dynamic_slice_in_dim(causal_filter_weight, tp_index * delta_cols, delta_cols, 2)
    rate_logarithm = lax.dynamic_slice_in_dim(
        head_decay_logrates, tp_index * head_count, head_count
    )
    shift_amounts = lax.dynamic_slice_in_dim(decay_input_shift, tp_index * head_count, head_count)
    strength_offsets = lax.dynamic_slice_in_dim(strength_shift, tp_index * head_count, head_count)
    beta = jax.nn.sigmoid(beta_raw.astype(jnp.float32) + strength_offsets)
    decay_logarithm = (
        -jnp.exp(rate_logarithm)
        * jax.nn.softplus(decay_unshaped.astype(jnp.float32) + shift_amounts)
        + decay_spike
    )
    out_local, out_reach, state = delta_pass(
        query_raw, key_raw, value_raw, *halos, taps, beta, decay_logarithm, head_depth
    )
    incoming = earlier_state(state, head_depth)
    delta_mixed = finish_pass(out_local, out_reach, incoming, head_norm_scale)
    group_ids = tp_index * groups_dev + jnp.arange(pool_cols) // GROUP_DIM
    positions = sp_index * tok_rows + jnp.arange(tok_rows)
    pool_diff = pool_means(previous_pool, pool_raw, group_ids, positions)
    local_mix = lax.dynamic_slice_in_dim(group_mixing_weight, tp_index * groups_dev, groups_dev, 0)
    pooled = jnp.einsum(
        "tgc,gcd->tgd",
        pool_diff.reshape(tok_rows, groups_dev, GROUP_DIM),
        local_mix,
        preferred_element_type=jnp.float32,
    )
    pool_scale = lax.dynamic_slice_in_dim(mean_channel_scale, tp_index * pool_cols, pool_cols)
    pool_mixed = (pooled.reshape(tok_rows, pool_cols) * pool_scale.astype(jnp.float32)).astype(
        jnp.bfloat16
    )
    mixed = jnp.concatenate([pool_mixed, delta_mixed], axis=1)
    pool_weight_rows, delta_weight_rows = (
        lax.all_gather(mean_output_weight, "sp", axis=1, tiled=True),
        lax.all_gather(delta_output_weight, "sp", axis=1, tiled=True),
    )
    out_weight = jnp.concatenate([pool_weight_rows, delta_weight_rows], axis=0)
    return lax.psum_scatter(
        jnp.dot(mixed, out_weight, preferred_element_type=jnp.float32).astype(jnp.bfloat16),
        "tp",
        scatter_dimension=0,
        tiled=True,
    )


def solution(mesh):
    return jax.shard_map(
        per_device,
        mesh=mesh,
        in_specs=(
            P("sp", None),
            P(),
            P("sp", "tp"),
            P("sp", "tp"),
            P("sp", "tp"),
            P("sp", "tp"),
            P("sp", "tp"),
            P("sp", "tp"),
            P(),
            P(),
            P(),
            P(),
            P("sp", "tp"),
            P(),
            P(),
            P(),
            P("tp", "sp"),
            P("tp", "sp"),
        ),
        out_specs=P(("sp", "tp"), None),
        check_vma=False,
    )
```

time: 769 us -> 565 us (0.73); the launches traced: 758 us -> 564 us
  matrix products: 246 us -> 65.1 us
  waiting for transfers between devices: 305 us -> 363 us
  other arithmetic: 52.1 us -> 18.7 us
  blocking collectives: 65.2 us -> 33 us
  Pallas kernels: 0 us -> 28.7 us
  local copies, waits for them, and re-layouts: 27.6 us -> 6.4 us
  starting transfers between devices: 45.1 us -> 35.7 us
    dot_general x120 -> x8, matrix products: 224 us -> 43.2 us  [the longest x5 42 us: per_device(): jnp.dot(normed, weight, preferred_element_type=F32).astype(BF16)]
    all_gather x1, waiting for transfers between devices: 0.01 us -> 75 us  [per_device(): lax.all_gather(delta_output_weight, 'sp', axis=1, tiled=True)]
    all_gather x4, waiting for transfers between devices: 214 us -> 176 us  [per_device(): gather = lambda weight: lax.all_gather(weight, 'sp', axis=0, tiled=True)]
    all_gather x2 -> x1, blocking collectives: 65.2 us -> 33 us  [per_device(): lax.all_gather(jnp.concatenate([strength_weight, decay_input_weight], axi...]
    pallas_call x0 -> x2, Pallas kernels: none -> 28.7 us  [the longest x1 24.2 us: delta_pass(): pl.pallas_call(lambda *refs: delta_kernel(heads, depth, chunk, *refs), gr...]
    all_gather x1, waiting for transfers between devices: 0.01 us -> 27.4 us  [per_device(): lax.all_gather(mean_output_weight, 'sp', axis=1, tiled=True)]
    mul x3 -> x0, other arithmetic: 15.6 us -> none  [the longest x1 7.26 us: block_terms(): keys_beta * jnp.exp(cumulative)[..., None]]
    ppermute x9 -> x8, starting transfers between devices: 44.8 us -> 35.4 us  [shifted_2(): return lax.ppermute(block, axis, route)]
  transfers between devices with their start and end apart: 16 -> 15, of which waited for: 11 -> 10; matrix products, arithmetic and copies ran while one was open for 41% -> 13% of each run, Pallas kernels for 0% -> 5%
where the time goes in v1:
time: 565 us; the launch traced here: 564 us
  waiting for transfers between devices  363 us (64%)
  matrix products  65.1 us (12%)
  starting transfers between devices  35.7 us (6%)
  blocking collectives  33 us (6%)
  Pallas kernels  28.7 us (5%)
  other arithmetic  18.7 us (3%)
  between operations  13.9 us (2%)
  local copies, waits for them, and re-layouts  6.4 us (1%)
    all_gather x4, waiting for transfers between devices, per_device(): gather = lambda weight: lax.all_gather(weight, 'sp', axis=0, tiled=True)  176 us
    all_gather x1, waiting for transfers between devices, per_device(): lax.all_gather(delta_output_weight, 'sp', axis=1, tiled=True)  75 us
    reduce_scatter x1, waiting for transfers between devices, per_device(): lax.psum_scatter(jnp.dot(mixed, out_weight, preferred_element_type=jnp.fl...  69.7 us
    dot_general x5, matrix products, per_device(): jnp.dot(normed, weight, preferred_element_type=F32).astype(BF16)  42 us
    ppermute x8, starting transfers between devices, shifted_2(): return lax.ppermute(block, axis, route)  35.4 us
    all_gather x1, blocking collectives, per_device(): lax.all_gather(jnp.concatenate([strength_weight, decay_input_weight], axi...  33 us
    all_gather x1, waiting for transfers between devices, per_device(): lax.all_gather(mean_output_weight, 'sp', axis=1, tiled=True)  27.4 us
    pallas_call x1, Pallas kernels, delta_pass(): pl.pallas_call(lambda *refs: delta_kernel(heads, depth, chunk, *refs), gr...  24.2 us
  transfers between devices with their start and end apart: 15, of which 10 were waited for; matrix products, arithmetic and copies ran while one was open for 13% of the time, Pallas kernels for 5%

profile of v1, /device:TPU:0, one launch (start us, length us, event | category | flops | bytes accessed | tf_op | source)
XLA Modules:
  0.0 564.2 jit_solution(11996877387421783596)
XLA Ops:
  10.8 5.1 fusion
  16.2 33.0 %all_gather.25 = bf16[4096,8]{0,1:T(8,128)(2,1)S(1)} all-gather(bf16[512,8]{0,1:T(8,128)(2,1)S(1)} %pad_maximum_fusion), channel_id=1, replica_groups=mesh['sp'=8,'tp'=4] {'sp'}, dimensions={0}, use_global_device_ids=true | all-gather | bytes 73728 | tf_op jit(solution)/shard_map/all_gather | solution.py:272
  50.9 10.4 %fusion.2 = bf16[1024,4096]{1,0:T(8,128)(2,1)} fusion(bf16[1024,4096]{1,0:T(8,128)(2,1)} %param.18, f32[4096]{0:T(1024)S(1)} %convert_element_type.72, f32[1024]{0:T(1024)S(1)} %add_rsqrt_fusion), kind=kLoop, calls=%fused_computation.4 | loop fusion | flops 16777216 | bytes 16797696 | tf_op jit(solution)/shard_map/convert_element_type | solution.py:271
  61.3 5.7 %convolution_convert_fusion.4 = bf16[1024,8]{1,0:T(8,128)(2,1)S(1)} fusion(bf16[1024,4096]{1,0:T(8,128)(2,1)} %fusion.2, bf16[4096,8]{0,1:T(8,128)(2,1)S(1)} %all_gather.25), kind=kOutput, calls=%fused_computation.53 | convolution fusion | flops 67117056 | bytes 8470528 | tf_op jit(solution)/shard_map/dot_general | solution.py:275
  67.6 17.9 %all-gather.9.cloned.1.call-done = bf16[4096,512]{1,0:T(8,128)(2,1)} async-done(((bf16[512,512]{1,0:T(8,128)(2,1)}), bf16[4096,512]{1,0:T(8,128)(2,1)}) %all-gather.9.cloned.1.call-update) | async-done | bytes 4194320 | tf_op jit(solution)/shard_map/all_gather | solution.py:276
  85.4 9.0 %convolution_convert_fusion.2.refs_0_ = bf16[1024,512]{1,0:T(8,128)(2,1)S(1)} fusion(bf16[1024,4096]{1,0:T(8,128)(2,1)} %fusion.2, bf16[4096,512]{1,0:T(8,128)(2,1)} %all-gather.9.cloned.1.call-done), kind=kOutput, calls=%fused_computation.50 | convolution fusion | flops 4295491584 | bytes 13631488 | tf_op jit(solution)/shard_map/dot_general | solution.py:275
  94.5 2.6 collective-permute-start.1
  97.2 62.0 %all-gather.11.cloned.1.call-done = bf16[4096,512]{1,0:T(8,128)(2,1)} async-done(((bf16[512,512]{1,0:T(8,128)(2,1)}), bf16[4096,512]{1,0:T(8,128)(2,1)}) %all-gather.11.cloned.1.call-update) | async-done | bytes 4194320 | tf_op jit(solution)/shard_map/all_gather | solution.py:276
  159.1 9.1 %convolution_convert_fusion.1.refs_1_ = bf16[1024,512]{1,0:T(8,128)(2,1)S(1)} fusion(bf16[1024,4096]{1,0:T(8,128)(2,1)} %fusion.2, bf16[4096,512]{1,0:T(8,128)(2,1)} %all-gather.11.cloned.1.call-done), kind=kOutput, calls=%fused_computation.49 | convolution fusion | flops 4295491584 | bytes 13631488 | tf_op jit(solution)/shard_map/dot_general | solution.py:275
  169.2 2.4 collective-permute-start.2
  171.6 61.2 %all-gather.13.cloned.1.call-done = bf16[4096,512]{1,0:T(8,128)(2,1)} async-done(((bf16[512,512]{1,0:T(8,128)(2,1)}), bf16[4096,512]{1,0:T(8,128)(2,1)}) %all-gather.13.cloned.1.call-update) | async-done | bytes 4194320 | tf_op jit(solution)/shard_map/all_gather | solution.py:276
  232.8 9.1 %convolution_convert_fusion.refs_2_ = bf16[1024,512]{1,0:T(8,128)(2,1)S(1)} fusion(bf16[1024,4096]{1,0:T(8,128)(2,1)} %fusion.2, bf16[4096,512]{1,0:T(8,128)(2,1)} %all-gather.13.cloned.1.call-done), kind=kOutput, calls=%fused_computation.48 | convolution fusion | flops 4295491584 | bytes 13631488 | tf_op jit(solution)/shard_map/dot_general | solution.py:275
  242.0 2.5 collective-permute-start.3
  244.5 1.4 collective-permute-done.3.refs_5_
  245.9 24.2 %shard_map.172 = (f32[1024,512]{1,0:T(8,128)S(1)}, bf16[1024,512]{1,0:T(8,128)(2,1)S(1)}, f32[4,128,256]{2,1,0:T(8,128)S(1)}) custom-call(bf16[1024,512]{1,0:T(8,128)(2,1)S(1)} %convolution_convert_fusion.2.refs_0_, bf16[1024,512]{1,0:T(8,128)(2,1)S(1)} %copy-done.5, bf16[1024,512]{1,0:T(8,128)(2,1)S(1)} %convolution_convert_fusion.refs_2_, ...), custom_call_target="tpu_custom_call" | custom-call | flops 2147483648 | bytes 6291456 | tf_op jit(solution)/shard_map/pallas_call | solution.py:167
  270.1 1.3 copy-done.2
  272.4 4.4 collective-permute-start.4
  276.8 35.1 %all-gather.7.cloned.1.call-done = bf16[4096,512]{1,0:T(8,128)(2,1)} async-done(((bf16[512,512]{1,0:T(8,128)(2,1)}), bf16[4096,512]{1,0:T(8,128)(2,1)}) %all-gather.7.cloned.1.call-update) | async-done | bytes 4194320 | tf_op jit(solution)/shard_map/all_gather | solution.py:276
  311.9 9.1 %convolution_convert_fusion.3 = bf16[1024,512]{1,0:T(8,128)(2,1)S(1)} fusion(bf16[1024,4096]{1,0:T(8,128)(2,1)} %fusion.2, bf16[4096,512]{1,0:T(8,128)(2,1)} %all-gather.7.cloned.1.call-done), kind=kOutput, calls=%fused_computation.51 | convolution fusion | flops 4295491584 | bytes 13631488 | tf_op jit(solution)/shard_map/dot_general | solution.py:275
  321.0 2.6 collective-permute-start
  323.6 4.0 collective-permute-start.5
  328.0 4.7 collective-permute-done.5
  332.9 10.4 %collective-permute-start.6 = (bf16[4,128,256]{2,1,0:T(8,128)(2,1)S(1)}, bf16[4,128,256]{2,1,0:T(8,128)(2,1)S(1)}, u32[]{:S(2)}, u32[]{:S(2)}) collective-permute-start(bf16[4,128,256]{2,1,0:T(8,128)(2,1)S(1)} %fusion.31), channel_id=1, source_target_pairs={{0,8},{4,12},{8,16},{12,20},{16,24},{20,28},{1,9},{5,13},{9,17},{1... | collective-permute-start | bytes 786440 | tf_op jit(solution)/shard_map/ppermute | solution.py:20
  343.3 8.2 %fusion.32 = f32[4,128,1024]{2,1,0:T(8,128)} fusion(bf16[16,128,128]{2,1,0:T(8,128)(2,1)S(1)} %copy-done, s32[]{:T(128)S(6)} %select_n.179, s32[512]{0:T(512)S(1)} %fusion.50, s32[1024]{0:T(1024)S(1)} %add_add_fusion, f32[1039,512]{1,0:T(8,128)S(1)} %maximum_convert_fusion, pred[512]{0:T(512)(128)(4,1)S(1)} %get-tuple-element.13, ...), kind=kOutput, calls=%fused_computation.56 | convolution fusion | flops 153092096 | bytes 35796996 | tf_op jit(solution)/shard_map/tgc,gcd->tgd/dot_general | solution.py:310
  351.5 1.9 copy.35
  353.7 6.5 %collective-permute-start.7 = (bf16[4,128,128]{2,1,0:T(8,128)(2,1)S(1)}, bf16[4,128,128]{2,1,0:T(8,128)(2,1)S(1)}, u32[]{:S(2)}, u32[]{:S(2)}) collective-permute-start(bf16[4,128,128]{2,1,0:T(8,128)(2,1)S(1)} %slice.136), channel_id=1, source_target_pairs={{0,16},{4,20},{8,24},{12,28},{1,17},{5,21},{9,25},{13,29},{2,18},{... | collective-permute-start | bytes 393224 | tf_op jit(solution)/shard_map/ppermute | solution.py:20
  361.5 4.7 collective-permute-done.7
  367.0 4.6 shard_map.173
  371.6 27.4 %all-gather.15.cloned.1.call-done = bf16[512,4096]{1,0:T(8,128)(2,1)} async-done(((bf16[512,512]{1,0:T(8,128)(2,1)}), bf16[512,4096]{1,0:T(8,128)(2,1)}) %all-gather.15.cloned.1.call-update) | async-done | bytes 4194320 | tf_op jit(solution)/shard_map/all_gather | solution.py:322
  399.0 75.0 %all-gather.17.cloned.1.call-done = bf16[512,4096]{1,0:T(8,128)(2,1)} async-done(((bf16[512,512]{1,0:T(8,128)(2,1)}), bf16[512,4096]{1,0:T(8,128)(2,1)}) %all-gather.17.cloned.1.call-update) | async-done | bytes 4194320 | tf_op jit(solution)/shard_map/all_gather | solution.py:323
  474.0 13.6 %fusion.7 = bf16[1024,4096]{1,0:T(8,128)(2,1)} fusion(bf16[512,4096]{1,0:T(8,128)(2,1)} %all-gather.17.cloned.1.call-done, bf16[512,4096]{1,0:T(8,128)(2,1)} %all-gather.15.cloned.1.call-done, bf16[1024,512]{1,0:T(8,128)(2,1)} %shard_map.173, bf16[1024,512]{1,0:T(8,128)(2,1)S(1)} %copy-done.6), kind=kOutput, calls=%fused_computation.9 | convolution fusion | flops 8615100416 | bytes 18874368 | tf_op jit(solution)/shard_map/dot_general | solution.py:327
  487.6 69.7 %reduce-scatter.2.cloned.1.call-done = bf16[256,4096]{1,0:T(8,128)(2,1)} async-done(((bf16[1024,4096]{1,0:T(8,128)(2,1)}), bf16[256,4096]{1,0:T(8,128)(2,1)}) %reduce-scatter.2.cloned.1.call-update) | async-done | bytes 2097168 | tf_op jit(solution)/shard_map/reduce_scatter | solution.py:326
  (80 shorter events, 11.5 us)
Async XLA Ops:
  6.5 336.8 %copy-start = (bf16[16,128,128]{2,1,0:T(8,128)(2,1)S(1)}, bf16[16,128,128]{2,1,0:T(8,128)(2,1)}, u32[]{:S(2)}) copy-start(bf16[16,128,128]{2,1,0:T(8,128)(2,1)} %param.32) | copy-start | bytes 1572868
  6.5 4.1 copy-start.8
  6.5 78.9 %all-gather.9.cloned.1.call-start = ((), (), s32[]{:S(2)}) async-start(), calls=%async_computation.2 | async-start | bytes 4718592 | tf_op jit(solution)/shard_map/all_gather | solution.py:276
  7.3 151.9 %all-gather.11.cloned.1.call-start = ((), (), s32[]{:S(2)}) async-start(), calls=%async_computation.3 | async-start | bytes 4718592 | tf_op jit(solution)/shard_map/all_gather | solution.py:276
  8.0 224.8 %all-gather.13.cloned.1.call-start = ((), (), s32[]{:S(2)}) async-start(), calls=%async_computation.4 | async-start | bytes 4718592 | tf_op jit(solution)/shard_map/all_gather | solution.py:276
  8.7 303.2 %all-gather.7.cloned.1.call-start = ((), (), s32[]{:S(2)}) async-start(), calls=%async_computation.1 | async-start | bytes 4718592 | tf_op jit(solution)/shard_map/all_gather | solution.py:276
  9.3 389.7 %all-gather.15.cloned.1.call-start = ((), (), s32[]{:S(2)}) async-start(), calls=%async_computation.5 | async-start | bytes 4718592 | tf_op jit(solution)/shard_map/all_gather | solution.py:322
  9.9 464.1 %all-gather.17.cloned.1.call-start = ((), (), s32[]{:S(2)}) async-start(), calls=%async_computation.6 | async-start | bytes 4718592 | tf_op jit(solution)/shard_map/all_gather | solution.py:323
  10.5 546.9 %reduce-scatter.2.cloned.1.call-start = ((), (), s32[]{:S(2)}) async-start(), calls=%async_computation.7 | async-start | bytes 10485760 | tf_op jit(solution)/shard_map/reduce_scatter | solution.py:326
  10.7 5.2 copy-start.11
  10.7 5.3 copy-start.12
  10.7 5.3 copy-start.13
  10.7 5.4 copy-start.9
  10.7 5.4 copy-start.10
  10.7 38.4 %copy-start.7 = (f32[1024,4]{0,1:T(4,128)S(1)}, f32[1024,4]{0,1:T(4,128)}, u32[]{:S(2)}) copy-start(f32[1024,4]{0,1:T(4,128)} %param.30) | copy-start | bytes 49156
  94.5 150.0 %collective-permute-start.1 = (bf16[8,512]{1,0:T(8,128)(2,1)S(1)}, bf16[8,512]{1,0:T(8,128)(2,1)S(1)}, u32[]{:S(2)}, u32[]{:S(2)}) collective-permute-start(bf16[8,512]{1,0:T(8,128)(2,1)S(1)} %slice.129), channel_id=1, source_target_pairs={{0,4},{4,8},{8,12},{12,16},{16,20},{20,24},{24,28},{1,5},{5,9},{9,... | collective-permute-start | bytes 24584 | tf_op jit(solution)/shard_map/ppermute | solution.py:20
  168.2 1.0 copy-start.4
  169.2 75.3 %collective-permute-start.2 = (bf16[8,512]{1,0:T(8,128)(2,1)S(1)}, bf16[8,512]{1,0:T(8,128)(2,1)S(1)}, u32[]{:S(2)}, u32[]{:S(2)}) collective-permute-start(bf16[8,512]{1,0:T(8,128)(2,1)S(1)} %slice.130), channel_id=1, source_target_pairs={{0,4},{4,8},{8,12},{12,16},{16,20},{20,24},{24,28},{1,5},{5,9},{9,... | collective-permute-start | bytes 24584 | tf_op jit(solution)/shard_map/ppermute | solution.py:20
  232.8 13.1 %copy-start.5 = (bf16[1024,512]{1,0:T(8,128)(2,1)S(1)}, bf16[1024,512]{1,0:T(8,128)(2,1)}, u32[]{:S(2)}) copy-start(bf16[1024,512]{1,0:T(8,128)(2,1)} %copy-done.4) | copy-start | bytes 3145732
  242.0 3.9 collective-permute-start.3
  270.0 1.3 copy-start.2
  271.4 1.0 copy-start.3
  272.4 51.2 %collective-permute-start.4 = (bf16[4,128,256]{2,1,0:T(8,128)(2,1)S(1)}, bf16[4,128,256]{2,1,0:T(8,128)(2,1)S(1)}, u32[]{:S(2)}, u32[]{:S(2)}) collective-permute-start(bf16[4,128,256]{2,1,0:T(8,128)(2,1)S(1)} %convert_element_type.86), channel_id=1, source_target_pairs={{0,4},{4,8},{8,12},{12,16},{16,20},{20,24},{24,28},{1,5},{5,9},{9,... | collective-permute-start | bytes 786440 | tf_op jit(solution)/shard_map/ppermute | solution.py:20
  321.0 11.7 %copy-start.14 = (pred[256]{0:T(512)(128)(4,1)S(1)}, pred[256]{0:T(512)(128)(4,1)}, u32[]{:S(2)}) copy-start(pred[256]{0:T(512)(128)(4,1)} %constant.125.clone.1) | copy-start | bytes 772
  321.0 6.6 %collective-permute-start = (bf16[15,512]{1,0:T(8,128)(2,1)S(1)}, bf16[15,512]{1,0:T(8,128)(2,1)S(1)}, u32[]{:S(2)}, u32[]{:S(2)}) collective-permute-start(bf16[15,512]{1,0:T(8,128)(2,1)S(1)} %slice.112), channel_id=1, source_target_pairs={{0,4},{4,8},{8,12},{12,16},{16,20},{20,24},{24,28},{1,5},{5,9},{9,... | collective-permute-start | bytes 46088 | tf_op jit(solution)/shard_map/ppermute | solution.py:20
  323.6 9.0 %collective-permute-start.5 = (bf16[4,128,256]{2,1,0:T(8,128)(2,1)S(1)}, bf16[4,128,256]{2,1,0:T(8,128)(2,1)S(1)}, u32[]{:S(2)}, u32[]{:S(2)}) collective-permute-start(bf16[4,128,256]{2,1,0:T(8,128)(2,1)S(1)} %collective-permute-done.4), channel_id=1, source_target_pairs={{0,4},{4,8},{8,12},{12,16},{16,20},{20,24},{24,28},{1,5},{5,9},{9,... | collective-permute-start | bytes 786440 | tf_op jit(solution)/shard_map/ppermute | solution.py:20
  332.9 20.6 %collective-permute-start.6 = (bf16[4,128,256]{2,1,0:T(8,128)(2,1)S(1)}, bf16[4,128,256]{2,1,0:T(8,128)(2,1)S(1)}, u32[]{:S(2)}, u32[]{:S(2)}) collective-permute-start(bf16[4,128,256]{2,1,0:T(8,128)(2,1)S(1)} %fusion.31), channel_id=1, source_target_pairs={{0,8},{4,12},{8,16},{12,20},{16,24},{20,28},{1,9},{5,13},{9,17},{1... | collective-permute-start | bytes 786440 | tf_op jit(solution)/shard_map/ppermute | solution.py:20
  353.7 12.5 %collective-permute-start.7 = (bf16[4,128,128]{2,1,0:T(8,128)(2,1)S(1)}, bf16[4,128,128]{2,1,0:T(8,128)(2,1)S(1)}, u32[]{:S(2)}, u32[]{:S(2)}) collective-permute-start(bf16[4,128,128]{2,1,0:T(8,128)(2,1)S(1)} %slice.136), channel_id=1, source_target_pairs={{0,16},{4,20},{8,24},{12,28},{1,17},{5,21},{9,25},{13,29},{2,18},{... | collective-permute-start | bytes 393224 | tf_op jit(solution)/shard_map/ppermute | solution.py:20
  367.0 107.0 %copy-start.6 = (bf16[1024,512]{1,0:T(8,128)(2,1)S(1)}, bf16[1024,512]{1,0:T(8,128)(2,1)}, u32[]{:S(2)}) copy-start(bf16[1024,512]{1,0:T(8,128)(2,1)} %multiply_convert_fusion) | copy-start | bytes 3145732
  487.6 69.7 %copy-start.1 = (bf16[16,128,128]{2,1,0:T(8,128)(2,1)S(1)}, bf16[16,128,128]{2,1,0:T(8,128)(2,1)}, u32[]{:S(2)}) copy-start(bf16[16,128,128]{2,1,0:T(8,128)(2,1)} %param.32) | copy-start | bytes 1572868
Sparse Core Ops, SparseCore 0:
  9.5 75.9 all-gather.8
  87.6 71.5 all-gather.10
  161.3 71.4 all-gather.12
  234.8 77.1 all-gather.6
  313.8 85.0 all-gather.14
  400.9 73.0 all-gather.16
  487.8 69.5 reduce-scatter.1
